TPU v7x, 32 devices: a whole 2x2x4 slice. The times are simulated.
32 devices in a mesh: fs: 8 (over z, y), tp: 4 (over x, core).
Axes of the slice: x: 2, y: 2, z: 4, core: 2. Of those that a mesh axis runs over, the one named last changes fastest.
Arguments:
- prompt: bfloat16 [4096, 2048], P(('fs', 'tp')), may hold values from -6 to 6
- norm_gain: float32 [2048], P('fs'), may hold values from 0.1 to 1.9
- up_trained: float32 [2048, 8192], P('fs', 'tp'), may hold values from -0.125 to 0.125
- down_trained: float32 [2048, 8192], P('fs', 'tp'), may hold values from -0.0625 to 0.0625
Outputs:
- up_served: bfloat16 [2048, 8192], P(None, 'tp')
- down_served: bfloat16 [8192, 2048], P('tp')
- mixed: bfloat16 [4096, 2048], P(('fs', 'tp'))
All inputs are finite; a program needn't handle non-finite values.
Results may differ from a plain program's by a relative error of at most 0.014.
Values may be sent and summed in bfloat16 or wider, within the bound.
A program may use at most 128 MiB of HBM per device.

v0:
```python
import jax
import jax.numpy as jnp
from jax import lax
from jax.sharding import PartitionSpec as P


def shards(prompt, norm_gain, up_trained, down_trained):
    up_local = (norm_gain[:, None] * up_trained).astype(jnp.bfloat16)
    down_local = down_trained.astype(jnp.bfloat16)
    values = prompt.astype(jnp.float32)
    scale = lax.rsqrt(jnp.mean(values * values, axis=-1, keepdims=True) + 1e-06)
    normed = (values * scale).astype(jnp.bfloat16)
    group_rows = lax.all_gather(normed, "tp", axis=0, tiled=True)
    pieces = (
        lax.all_gather(up_local, "fs", axis=0, tiled=True),
        lax.all_gather(down_local, "fs", axis=0, tiled=True),
    )
    pre = jnp.dot(group_rows, pieces[0], preferred_element_type=jnp.float32)
    up_buffer = pieces[0]
    down_buffer = pieces[1]
    pre, up_whole, down_whole = (pre, up_buffer, down_buffer)
    hidden = jnp.square(jax.nn.relu(pre)).astype(jnp.bfloat16)
    down_served = jnp.transpose(down_whole)
    mixed = lax.psum_scatter(
        jnp.dot(hidden, down_served, preferred_element_type=jnp.float32).astype(jnp.bfloat16),
        "tp",
        scatter_dimension=0,
        tiled=True,
    )
    return (up_whole, down_served, mixed)


def solution(mesh):
    return jax.shard_map(
        shards,
        mesh=mesh,
        in_specs=(P(("fs", "tp"), None), P("fs"), P("fs", "tp"), P("fs", "tp")),
        out_specs=(P(None, "tp"), P("tp", None), P(("fs", "tp"), None)),
        check_vma=False,
    )
```

profile of v0, /device:TPU:1, one launch (start us, length us, event | category | flops | bytes accessed | tf_op | source)
XLA Modules:
  0.0 357.7 jit_solution(13753829205279300968)
XLA Ops:
  7.2 0.0 copy-start
  7.2 0.0 all-gather.8.cloned.1.call-start
  7.2 1.4 fusion
  8.6 2.0 fusion.1
  10.6 0.0 all-gather.8.cloned.1.call-update
  10.6 0.0 all-gather.4.cloned.1.call-start
  10.7 2.7 multiply_convert_fusion.1
  13.4 0.0 all-gather.4.cloned.1.call-update
  13.4 0.0 all-gather.6.cloned.1.call-start
  13.5 0.0 copy-done
  13.5 1.4 copy.7
  14.9 0.0 all-gather.6.cloned.1.call-update
  14.9 0.0 reduce-scatter.2.cloned.1.call-start
  14.9 20.9 %all-gather.8.cloned.1.call-done = bf16[512,2048]{1,0:T(8,128)(2,1)} async-done(((bf16[128,2048]{1,0:T(8,128)(2,1)}), bf16[512,2048]{1,0:T(8,128)(2,1)}) %all-gather.8.cloned.1.call-update) | async-done | bytes 2097168 | tf_op jit(solution)/shard_map/all_gather | solution.py:13
  35.8 126.1 %all-gather.4.cloned.1.call-done = bf16[2048,2048]{1,0:T(8,128)(2,1)} async-done(((bf16[256,2048]{1,0:T(8,128)(2,1)}), bf16[2048,2048]{1,0:T(8,128)(2,1)}) %all-gather.4.cloned.1.call-update) | async-done | bytes 8388624 | tf_op jit(solution)/shard_map/all_gather | solution.py:15
  161.9 125.7 %all-gather.6.cloned.1.call-done = bf16[2048,2048]{0,1:T(8,128)(2,1)} async-done(((bf16[256,2048]{0,1:T(8,128)(2,1)}), bf16[2048,2048]{0,1:T(8,128)(2,1)}) %all-gather.6.cloned.1.call-update) | async-done | bytes 8388624 | tf_op jit(solution)/shard_map/all_gather | solution.py:16
  287.6 16.5 %convolution_convert_fusion = bf16[512,2048]{1,0:T(8,128)(2,1)} fusion(bf16[2048,2048]{0,1:T(8,128)(2,1)} %all-gather.6.cloned.1.call-done, bf16[512,2048]{1,0:T(8,128)(2,1)} %all-gather.8.cloned.1.call-done, bf16[2048,2048]{1,0:T(8,128)(2,1)} %all-gather.4.cloned.1.call-done), kind=kOutput, calls=%fused_computation.1 | convolution fusion | flops 8594128896 | bytes 20971520 | tf_op jit(solution)/shard_map/dot_general | solution.py:25
  304.1 0.0 reduce-scatter.2.cloned.1.call-update
  304.1 30.1 %reduce-scatter.2.cloned.1.call-done = bf16[128,2048]{1,0:T(8,128)(2,1)} async-done(((bf16[512,2048]{1,0:T(8,128)(2,1)}), bf16[128,2048]{1,0:T(8,128)(2,1)}) %reduce-scatter.2.cloned.1.call-update) | async-done | bytes 524304 | tf_op jit(solution)/shard_map/reduce_scatter | solution.py:24
  334.2 8.4 %copy.10 = bf16[2048,2048]{1,0:T(8,128)(2,1)} copy(bf16[2048,2048]{1,0:T(8,128)(2,1)} %all-gather.4.cloned.1.call-done) | data formatting | bytes 16777216
  342.7 8.4 %copy.11 = bf16[2048,2048]{1,0:T(8,128)(2,1)} copy(bf16[2048,2048]{1,0:T(8,128)(2,1)} %bitcast.4) | data formatting | bytes 16777216
  (1 shorter events, 0.0 us)
Async XLA Ops:
  7.2 6.3 %copy-start = (f32[256,2048]{1,0:T(8,128)S(1)}, f32[256,2048]{1,0:T(8,128)}, u32[]{:S(2)}) copy-start(f32[256,2048]{1,0:T(8,128)} %param.7) | copy-start | bytes 6291460
  7.2 28.6 %all-gather.8.cloned.1.call-start = ((), (), s32[]{:S(2)}) async-start(), calls=%async_computation.3 | async-start | bytes 2621440 | tf_op jit(solution)/shard_map/all_gather | solution.py:13
  10.6 151.3 %all-gather.4.cloned.1.call-start = ((), (), s32[]{:S(2)}) async-start(), calls=%async_computation.1 | async-start | bytes 9437184 | tf_op jit(solution)/shard_map/all_gather | solution.py:15
  13.4 274.2 %all-gather.6.cloned.1.call-start = ((), (), s32[]{:S(2)}) async-start(), calls=%async_computation.2 | async-start | bytes 9437184 | tf_op jit(solution)/shard_map/all_gather | solution.py:16
  14.9 319.4 %reduce-scatter.2.cloned.1.call-start = ((), (), s32[]{:S(2)}) async-start(), calls=%async_computation.4 | async-start | bytes 2621440 | tf_op jit(solution)/shard_map/reduce_scatter | solution.py:24
Sparse Core Ops, SparseCore 0:
  10.7 25.0 all-gather.7
  38.5 123.3 all-gather.3
  164.5 123.0 all-gather.5
  304.3 29.9 reduce-scatter.1
where the time goes:
time: 359 us; the launch traced here: 358 us
  waiting for transfers between devices  303 us (84%)
  local copies, waits for them, and re-layouts  18.3 us (5%)
  matrix products  16.5 us (5%)
  between operations  13.8 us (4%)
  other arithmetic  6.11 us (2%)
    all_gather x1, waiting for transfers between devices, shards(): lax.all_gather(up_local, 'fs', axis=0, tiled=True)  126 us
    all_gather x1, waiting for transfers between devices, shards(): lax.all_gather(down_local, 'fs', axis=0, tiled=True)  126 us
    reduce_scatter x1, waiting for transfers between devices, shards(): lax.psum_scatter(jnp.dot(hidden, down_served, preferred_element_type=jnp....  30.1 us
    all_gather x1, waiting for transfers between devices, shards(): group_rows = lax.all_gather(normed, 'tp', axis=0, tiled=True)  20.9 us
    unnamed x5, local copies, waits for them, and re-layouts  18.3 us
    dot_general x1, matrix products, shards(): jnp.dot(hidden, down_served, preferred_element_type=jnp.float32)  16.5 us
  transfers between devices with their start and end apart: 4, of which 4 were waited for; matrix products, arithmetic and copies ran while one was open for 1% of the time, Pallas kernels for 0%

commit v1 on v0

v1 whole, which is shorter than its diff:
```python
import functools

import jax
import jax.numpy as jnp
from jax import lax
from jax.experimental import pallas as pl
from jax.experimental.pallas import tpu as pltpu
from jax.sharding import PartitionSpec as P

MESH = pl.DeviceIdType.MESH
PIECES = 2


def factor(fs):
    ny = 1
    while ny * 2 * ny * 2 <= fs:
        ny *= 2
    return fs // ny, ny


def kernel(nz, ny, tp, prompt, gain, up_f, down_f, up_out, down_out, mixed,
           up_all, down_all, norm_all, hidden, part_send, part_recv,
           w_send, w_recv, n_send, n_recv, p_send, p_recv, l_sem):
    fs = nz * ny
    rows, width = up_f.shape
    piece = rows // PIECES
    tokens = prompt.shape[0]
    me = lax.axis_index("fs")
    t = lax.axis_index("tp")
    z, y = me // ny, lax.rem(me, ny)
    exists = (z < nz - 1, z > 0, y < ny - 1, y > 0)
    step = (ny, -ny, 1, -1)
    trick = ny == 2 and nz % 2 == 0
    half = PIECES // 2
    even = lax.rem(z, 2) == 0
    mate = z + 1 - 2 * lax.rem(z, 2)
    buffers = (up_all, down_all)
    sent = []

    barrier = pltpu.get_barrier_semaphore()
    for direction in range(4):
        @pl.when(exists[direction])
        def _():
            pl.semaphore_signal(barrier, inc=1, device_id={"fs": me + step[direction]}, device_id_type=MESH)
    for offset in range(1, tp):
        pl.semaphore_signal(barrier, inc=1, device_id={"tp": lax.rem(t + offset, tp)}, device_id_type=MESH)

    def weights(phase, block, c, direction):
        start = pl.multiple_of(block * rows + c * piece, piece)
        ref = buffers[phase].at[pl.ds(start, piece)]
        slot = (phase * fs + block) * PIECES + c
        return pltpu.make_async_remote_copy(
            src_ref=ref, dst_ref=ref,
            send_sem=w_send.at[direction, slot], recv_sem=w_recv.at[slot],
            device_id={"fs": me + step[direction]}, device_id_type=MESH)

    def send(condition, phase, block, c, direction):
        condition = jnp.logical_and(condition, exists[direction])
        sent.append((condition, phase, block, c, direction))

        @pl.when(condition)
        def _():
            weights(phase, block, c, direction).start()

    def arrive(condition, phase, block, c):
        @pl.when(condition)
        def _():
            weights(phase, block, c, 0).wait_recv()

    for c in range(PIECES):
        where = pl.ds(pl.multiple_of(me * rows + c * piece, piece), piece)
        part = slice(c * piece, (c + 1) * piece)
        up_all[where, :] = (gain[part, :] * up_f[part, :]).astype(jnp.bfloat16)
    pl.semaphore_wait(barrier, sum(e.astype(jnp.int32) for e in exists) + tp - 1)
    always = z >= 0
    for c in range(PIECES):
        for direction in range(4):
            send(always, 0, me, c, direction)

    values = prompt[...].astype(jnp.float32)
    scale = lax.rsqrt(jnp.mean(values * values, axis=-1, keepdims=True) + 1e-06)
    mine = pl.ds(pl.multiple_of(t * tokens, tokens), tokens)
    norm_all[mine, :] = (values * scale).astype(jnp.bfloat16)
    for c in range(PIECES):
        where = pl.ds(pl.multiple_of(me * rows + c * piece, piece), piece)
        part = slice(c * piece, (c + 1) * piece)
        down_all[where, :] = down_f[part, :].astype(jnp.bfloat16)

    def token_copy(offset):
        return pltpu.make_async_remote_copy(
            src_ref=norm_all.at[mine], dst_ref=norm_all.at[mine],
            send_sem=n_send.at[offset], recv_sem=n_recv.at[t],
            device_id={"tp": lax.rem(t + offset, tp)}, device_id_type=MESH)

    def token_arrival(offset):
        source = lax.rem(t + offset, tp)
        ref = norm_all.at[pl.ds(pl.multiple_of(source * tokens, tokens), tokens)]
        return pltpu.make_async_remote_copy(
            src_ref=ref, dst_ref=ref, send_sem=n_send.at[offset], recv_sem=n_recv.at[source],
            device_id={"tp": source}, device_id_type=MESH)

    for offset in range(1, tp):
        token_copy(offset).start()
    for c in range(half):
        for direction in (2, 3):
            send(always, 1, me, c, direction)

    def own_down(d):
        for c in range(PIECES):
            send(z == d, 1, me, c, 0)
            send(z == nz - 1 - d, 1, me, c, 1)

    def column(phase, d):
        for c in range(PIECES):
            for s in (1, -1):
                zb = z + s * d
                there = jnp.logical_and(zb >= 0, zb < nz)
                block = zb * ny + y
                arrive(there, phase, block, c)
                send(there, phase, block, c, 1 if s > 0 else 0)
                across = there
                if trick and c >= half:
                    across = jnp.logical_and(there, zb != mate)
                send(across, phase, block, c, 2)
                send(across, phase, block, c, 3)

    def swap(phase):
        if not trick:
            return
        block = z * ny + 1 - y
        for c in range(half, PIECES):
            if phase == 0:
                arrive(always, phase, block, c)
            send(even, phase, block, c, 0)
            send(jnp.logical_not(even), phase, block, c, 1)

    def sideways(phase, d, s):
        zb = z + s * d
        inside = jnp.logical_and(zb >= 0, zb < nz)
        for e in range(1, ny):
            for u in (1, -1):
                yb = y + u * e
                there = jnp.logical_and(inside, jnp.logical_and(yb >= 0, yb < ny))
                for c in range(PIECES):
                    if trick and phase == 0 and d == 0 and c >= half:
                        continue
                    wanted = there
                    if trick and c >= half:
                        wanted = jnp.logical_and(there, zb != mate)
                    arrive(wanted, phase, zb * ny + yb, c)
                    if e < ny - 1:
                        send(wanted, phase, zb * ny + yb, c, 3 if u > 0 else 2)

    def swapped(phase):
        if trick:
            for c in range(half, PIECES):
                arrive(always, phase, mate * ny + 1 - y, c)

    def partial_copy(block, offset):
        peer = lax.rem(t + offset, tp)
        return pltpu.make_async_remote_copy(
            src_ref=part_send.at[block, pl.ds(pl.multiple_of(peer * tokens, tokens), tokens)],
            dst_ref=part_recv.at[t, block],
            send_sem=p_send.at[offset], recv_sem=p_recv.at[t],
            device_id={"tp": peer}, device_id_type=MESH)

    def consume(condition, block):
        @pl.when(condition)
        def _():
            where = pl.ds(pl.multiple_of(block * rows, rows), rows)
            pltpu.make_async_copy(down_all.at[where], down_out.at[where], l_sem.at[1]).start()
            part_send[block] = lax.dot_general(
                hidden[...], down_all[where, :], (((1,), (1,)), ((), ())),
                preferred_element_type=jnp.float32).astype(jnp.bfloat16)
            for offset in range(1, tp):
                partial_copy(block, offset).start()

    def consume_column(d):
        @pl.loop(0, 1 if d == 0 else 2)
        def _(i):
            zb = z + (1 - 2 * i) * d
            consume(jnp.logical_and(zb >= 0, zb < nz), zb * ny + y)

    def consume_sideways(d):
        @pl.loop(0, (1 if d == 0 else 2) * (ny - 1))
        def _(i):
            zb = z + (1 - 2 * (i // (ny - 1))) * d
            yb = lax.rem(y + 1 + lax.rem(i, ny - 1), ny)
            inside = jnp.logical_and(zb >= 0, zb < nz)
            if trick:
                inside = jnp.logical_and(inside, zb != mate)
            consume(inside, zb * ny + yb)

    def signs(d):
        return (1,) if d == 0 else (1, -1)

    own_down(0)
    for d in range(1, nz):
        column(0, d)
        if d == 1:
            swap(0)
        own_down(d)
    for c in range(half, PIECES):
        for direction in (2, 3):
            send(always, 1, me, c, direction)
    for d in range(nz):
        for s in signs(d):
            sideways(0, d, s)
    swapped(0)
    up_copy = pltpu.make_async_copy(up_all, up_out, l_sem.at[0])
    up_copy.start()
    for offset in range(1, tp):
        token_arrival(offset).wait_recv()
    tile = 256

    @pl.loop(0, width // tile)
    def _(j):
        at = pl.ds(pl.multiple_of(j * tile, tile), tile)
        pre = jnp.dot(norm_all[...], up_all[:, at], preferred_element_type=jnp.float32)
        hidden[:, at] = jnp.square(jnp.maximum(pre, 0.0)).astype(jnp.bfloat16)

    for d in range(1, nz):
        column(1, d)
        if d == nz - 1:
            swap(1)
        consume_column(d - 1)
        if d == 1:
            sideways(1, 0, 1)
            consume_sideways(0)
    if nz == 1:
        sideways(1, 0, 1)
        consume_sideways(0)
    consume_column(nz - 1)
    for d in range(1, nz):
        for s in signs(d):
            sideways(1, d, s)
        consume_sideways(d)
    if trick:
        swapped(1)
        consume(always, mate * ny + 1 - y)

    for offset in range(1, tp):
        source = lax.rem(t + offset, tp)
        whole = part_recv.at[source]
        arrival = pltpu.make_async_remote_copy(
            src_ref=whole, dst_ref=whole, send_sem=p_send.at[offset], recv_sem=p_recv.at[source],
            device_id={"tp": source}, device_id_type=MESH)
        arrival.wait_recv()
    for block in range(fs):
        total = part_send[block, mine, :].astype(jnp.float32)
        for offset in range(1, tp):
            total += part_recv[lax.rem(t + offset, tp), block].astype(jnp.float32)
        mixed[:, block * rows:(block + 1) * rows] = total.astype(jnp.bfloat16)

    for offset in range(1, tp):
        token_copy(offset).wait_send()
        whole = part_recv.at[t]
        pltpu.make_async_remote_copy(
            src_ref=whole, dst_ref=whole, send_sem=p_send.at[offset], recv_sem=p_recv.at[t],
            device_id={"tp": lax.rem(t + offset, tp)}, device_id_type=MESH).wait_send()
    for condition, phase, block, c, direction in sent:
        @pl.when(condition)
        def _():
            weights(phase, block, c, direction).wait_send()
    up_copy.wait()
    pltpu.make_async_copy(down_all, down_out, l_sem.at[1]).wait()


def solution(mesh):
    fs, tp = mesh.shape["fs"], mesh.shape["tp"]
    nz, ny = factor(fs)

    def shards(prompt, norm_gain, up_trained, down_trained):
        rows, width = up_trained.shape
        tokens, depth = prompt.shape
        bf16 = jnp.bfloat16
        slots = 2 * fs * PIECES
        any_space = pl.BlockSpec(memory_space=pl.ANY)
        vmem = pl.BlockSpec(memory_space=pltpu.VMEM)
        up_whole, down_whole, mixed = pl.pallas_call(
            functools.partial(kernel, nz, ny, tp),
            out_shape=(
                jax.ShapeDtypeStruct((depth, width), bf16),
                jax.ShapeDtypeStruct((depth, width), bf16),
                jax.ShapeDtypeStruct((tokens, depth), bf16),
            ),
            in_specs=[vmem] * 4,
            out_specs=(any_space, any_space, vmem),
            scratch_shapes=[
                pltpu.VMEM((depth, width), bf16),
                pltpu.VMEM((depth, width), bf16),
                pltpu.VMEM((tp * tokens, depth), bf16),
                pltpu.VMEM((tp * tokens, width), bf16),
                pltpu.VMEM((fs, tp * tokens, rows), bf16),
                pltpu.VMEM((tp, fs, tokens, rows), bf16),
                pltpu.SemaphoreType.DMA((4, slots)),
                pltpu.SemaphoreType.DMA((slots,)),
                pltpu.SemaphoreType.DMA((tp,)),
                pltpu.SemaphoreType.DMA((tp,)),
                pltpu.SemaphoreType.DMA((tp,)),
                pltpu.SemaphoreType.DMA((tp,)),
                pltpu.SemaphoreType.DMA((2,)),
            ],
            compiler_params=pltpu.CompilerParams(
                collective_id=0, has_side_effects=True, vmem_limit_bytes=60 * 1024 * 1024
            ),
        )(prompt, norm_gain[:, None], up_trained, down_trained)
        return up_whole, jnp.transpose(down_whole), mixed

    return jax.shard_map(
        shards,
        mesh=mesh,
        in_specs=(P(("fs", "tp"), None), P("fs"), P("fs", "tp"), P("fs", "tp")),
        out_specs=(P(None, "tp"), P("tp", None), P(("fs", "tp"), None)),
        check_vma=False,
    )
```

time: 359 us -> 199 us (0.55)
  waiting for transfers between devices: 303 us -> 0 us
  Pallas kernels: 0 us -> 175 us
  matrix products: 16.5 us -> 0 us
  between operations: 13.8 us -> 0.64 us
  other arithmetic: 6.11 us -> 0 us
  local copies, waits for them, and re-layouts: 18.3 us -> 23 us
    all_gather x3 -> x0, waiting for transfers between devices: 273 us -> none  [the longest x1 126 us: shards(): lax.all_gather(up_local, 'fs', axis=0, tiled=True)]
    pallas_call x0 -> x1, Pallas kernels: none -> 175 us  [shards(): pl.pallas_call(functools.partial(kernel, nz, ny, tp), out_shape=(jax.Shap...]
    reduce_scatter x1 -> x0, waiting for transfers between devices: 30.1 us -> none  [shards(): lax.psum_scatter(jnp.dot(hidden, down_served, preferred_element_type=jnp....]
    dot_general x1 -> x0, matrix products: 16.5 us -> none  [shards(): jnp.dot(hidden, down_served, preferred_element_type=jnp.float32)]
    convert_element_type x2 -> x0, other arithmetic: 4.74 us -> none  [the longest x1 2.74 us: shards(): up_local = (norm_gain[:, None] * up_trained).astype(jnp.bfloat16)]
  transfers between devices with their start and end apart: 4 -> 0, of which waited for: 4 -> 0; matrix products, arithmetic and copies ran while one was open for 1% -> 0% of each run, Pallas kernels for 0% -> 0%
where the time goes in v1:
time: 199 us
  Pallas kernels  175 us (88%)
  local copies, waits for them, and re-layouts  23 us (12%)
    pallas_call x1, Pallas kernels, shards(): pl.pallas_call(functools.partial(kernel, nz, ny, tp), out_shape=(jax.Shap...  175 us
    unnamed x5, local copies, waits for them, and re-layouts  21.5 us

profile of v1, /device:TPU:1, one launch (start us, length us, event | category | flops | bytes accessed | tf_op | source)
XLA Modules:
  0.0 198.6 jit_solution(568408266040467671)
XLA Ops:
  0.6 1.5 copy.8.gain
  2.1 175.0 %shard_map.67 = (bf16[2048,2048]{1,0:T(8,128)(2,1)}, bf16[2048,2048]{1,0:T(8,128)(2,1)}, bf16[128,2048]{1,0:T(8,128)(2,1)}) custom-call(bf16[128,2048]{1,0:T(8,128)(2,1)} %prompt.1, f32[256,1]{1,0:T(8,128)} %copy.8.gain, f32[256,2048]{1,0:T(8,128)} %up_f.1, f32[256,2048]{1,0:T(8,128)} %down_f.1), custom_call_target="tpu_custom_call" | custom-call | tf_op jit(solution)/shard_map/pallas_call | solution.py:280
  177.1 12.2 %copy.9 = bf16[2048,2048]{1,0:T(8,128)(2,1)} copy(bf16[2048,2048]{0,1:T(8,128)(2,1)} %bitcast.2) | data formatting | bytes 16777216
  189.3 0.0 copy-start
  189.3 8.5 %copy.12 = bf16[2048,2048]{1,0:T(8,128)(2,1)} copy(bf16[2048,2048]{1,0:T(8,128)(2,1)} %get-tuple-element.18) | data formatting | bytes 16777216
  197.8 0.0 copy-done
  197.8 0.8 copy.13
Async XLA Ops:
  189.3 8.5 %copy-start = (bf16[128,2048]{1,0:T(8,128)(2,1)S(1)}, bf16[128,2048]{1,0:T(8,128)(2,1)}, u32[]{:S(2)}) copy-start(bf16[128,2048]{1,0:T(8,128)(2,1)} %get-tuple-element.20) | copy-start | bytes 1572868

commit v2 on v1

--- a/solution.py
+++ b/solution.py
@@ -9,6 +9,7 @@
 
 MESH = pl.DeviceIdType.MESH
 PIECES = 2
+LIMIT = 40
 
 
 def factor(fs):
@@ -18,11 +19,29 @@
     return fs // ny, ny
 
 
-def kernel(nz, ny, tp, prompt, gain, up_f, down_f, up_out, down_out, mixed,
-           up_all, down_all, norm_all, hidden, part_send, part_recv,
-           w_send, w_recv, n_send, n_recv, p_send, p_recv, l_sem):
+def turns(rows):
+    return rows % 128 == 0
+
+
+def flush(up_in, down_in, mixed_in, up_out, down_out, mixed_out, sems):
+    copies = [
+        pltpu.make_async_copy(source, target, sems.at[i])
+        for i, (source, target) in enumerate(((up_in, up_out), (down_in, down_out), (mixed_in, mixed_out)))
+    ]
+    for copy in copies:
+        copy.start()
+    for copy in copies:
+        copy.wait()
+
+
+def kernel(nz, ny, tp, prompt, gain, up_f, down_f, up_all, down_out, mixed,
+           down_scratch, norm_all, hidden, part_send, part_recv,
+           w_send, w_recv, n_send, n_recv, p_send, p_recv):
     fs = nz * ny
     rows, width = up_f.shape
+    tile = 256
+    turned = turns(rows)
+    down_all = down_scratch if turned else down_out
     piece = rows // PIECES
     tokens = prompt.shape[0]
     me = lax.axis_index("fs")
@@ -168,12 +187,16 @@
         @pl.when(condition)
         def _():
             where = pl.ds(pl.multiple_of(block * rows, rows), rows)
-            pltpu.make_async_copy(down_all.at[where], down_out.at[where], l_sem.at[1]).start()
             part_send[block] = lax.dot_general(
                 hidden[...], down_all[where, :], (((1,), (1,)), ((), ())),
                 preferred_element_type=jnp.float32).astype(jnp.bfloat16)
             for offset in range(1, tp):
                 partial_copy(block, offset).start()
+            if turned:
+                @pl.loop(0, width // tile)
+                def _(j):
+                    at = pl.ds(pl.multiple_of(j * tile, tile), tile)
+                    down_out[at, where] = jnp.transpose(down_all[where, at])
 
     def consume_column(d):
         @pl.loop(0, 1 if d == 0 else 2)
@@ -207,11 +230,8 @@
         for s in signs(d):
             sideways(0, d, s)
     swapped(0)
-    up_copy = pltpu.make_async_copy(up_all, up_out, l_sem.at[0])
-    up_copy.start()
     for offset in range(1, tp):
         token_arrival(offset).wait_recv()
-    tile = 256
 
     @pl.loop(0, width // tile)
     def _(j):
@@ -262,8 +282,6 @@
         @pl.when(condition)
         def _():
             weights(phase, block, c, direction).wait_send()
-    up_copy.wait()
-    pltpu.make_async_copy(down_all, down_out, l_sem.at[1]).wait()
 
 
 def solution(mesh):
@@ -274,21 +292,22 @@
         rows, width = up_trained.shape
         tokens, depth = prompt.shape
         bf16 = jnp.bfloat16
+        turned = turns(rows)
+        down_shape = (width, depth) if turned else (depth, width)
         slots = 2 * fs * PIECES
         any_space = pl.BlockSpec(memory_space=pl.ANY)
         vmem = pl.BlockSpec(memory_space=pltpu.VMEM)
         up_whole, down_whole, mixed = pl.pallas_call(
             functools.partial(kernel, nz, ny, tp),
             out_shape=(
-                jax.ShapeDtypeStruct((depth, width), bf16),
-                jax.ShapeDtypeStruct((depth, width), bf16),
-                jax.ShapeDtypeStruct((tokens, depth), bf16),
+                pltpu.VMEM((depth, width), bf16),
+                pltpu.VMEM(down_shape, bf16),
+                pltpu.VMEM((tokens, depth), bf16),
             ),
             in_specs=[vmem] * 4,
-            out_specs=(any_space, any_space, vmem),
+            out_specs=[vmem] * 3,
             scratch_shapes=[
-                pltpu.VMEM((depth, width), bf16),
-                pltpu.VMEM((depth, width), bf16),
+                pltpu.VMEM((depth, width) if turned else (16, 128), bf16),
                 pltpu.VMEM((tp * tokens, depth), bf16),
                 pltpu.VMEM((tp * tokens, width), bf16),
                 pltpu.VMEM((fs, tp * tokens, rows), bf16),
@@ -299,13 +318,24 @@
                 pltpu.SemaphoreType.DMA((tp,)),
                 pltpu.SemaphoreType.DMA((tp,)),
                 pltpu.SemaphoreType.DMA((tp,)),
-                pltpu.SemaphoreType.DMA((2,)),
             ],
             compiler_params=pltpu.CompilerParams(
-                collective_id=0, has_side_effects=True, vmem_limit_bytes=60 * 1024 * 1024
+                collective_id=0, has_side_effects=True, vmem_limit_bytes=LIMIT * 1024 * 1024
             ),
         )(prompt, norm_gain[:, None], up_trained, down_trained)
-        return up_whole, jnp.transpose(down_whole), mixed
+        up_whole, down_whole, mixed = pl.pallas_call(
+            flush,
+            out_shape=(
+                jax.ShapeDtypeStruct((depth, width), bf16),
+                jax.ShapeDtypeStruct(down_shape, bf16),
+                jax.ShapeDtypeStruct((tokens, depth), bf16),
+            ),
+            in_specs=[vmem] * 3,
+            out_specs=[any_space] * 3,
+            scratch_shapes=[pltpu.SemaphoreType.DMA((3,))],
+            compiler_params=pltpu.CompilerParams(vmem_limit_bytes=2 * 1024 * 1024),
+        )(up_whole, down_whole, mixed)
+        return up_whole, down_whole if turned else jnp.transpose(down_whole), mixed
 
     return jax.shard_map(
         shards,

time: 199 us -> 183 us (0.920)
  local copies, waits for them, and re-layouts: 23 us -> 1.47 us
  Pallas kernels: 175 us -> 180 us
    unnamed x5 -> x0, local copies, waits for them, and re-layouts: 21.5 us -> none
    pallas_call x1 -> x2, Pallas kernels: 175 us -> 180 us  [the longest x1 174 us: shards(): pl.pallas_call(functools.partial(kernel, nz, ny, tp), out_shape=(pltpu.VM...]
where the time goes in v2:
time: 183 us
  Pallas kernels  180 us (98%)
    pallas_call x1, Pallas kernels, shards(): pl.pallas_call(functools.partial(kernel, nz, ny, tp), out_shape=(pltpu.VM...  174 us
    pallas_call x1, Pallas kernels, shards(): pl.pallas_call(flush, out_shape=(jax.ShapeDtypeStruct((depth, width), bf1...  6.19 us

profile of v2, /device:TPU:1, one launch (start us, length us, event | category | flops | bytes accessed | tf_op | source)
XLA Modules:
  0.0 182.6 jit_solution(16813299848783990574)
XLA Ops:
  0.6 1.5 copy.7.gain
  2.1 174.3 %shard_map.67 = (bf16[2048,2048]{1,0:T(8,128)(2,1)S(1)}, bf16[2048,2048]{1,0:T(8,128)(2,1)S(1)}, bf16[128,2048]{1,0:T(8,128)(2,1)S(1)}) custom-call(bf16[128,2048]{1,0:T(8,128)(2,1)} %prompt.1, f32[256,1]{1,0:T(8,128)} %copy.7.gain, f32[256,2048]{1,0:T(8,128)} %up_f.1, f32[256,2048]{1,0:T(8,128)} %down_f.1), custom_call_target="tpu_custom_call" | custom-call | tf_op jit(solution)/shard_map/pallas_call | solution.py:300
  176.4 6.2 %shard_map.68 = (bf16[2048,2048]{1,0:T(8,128)(2,1)}, bf16[2048,2048]{1,0:T(8,128)(2,1)}, bf16[128,2048]{1,0:T(8,128)(2,1)}) custom-call(bf16[2048,2048]{1,0:T(8,128)(2,1)S(1)} %get-tuple-element.6.up_in, bf16[2048,2048]{1,0:T(8,128)(2,1)S(1)} %get-tuple-element.7.down_in, bf16[128,2048]{1,0:T(8,128)(2,1)S(1)} %get-tuple-element.8.mixed_in), custom_call_target="tpu_custom_call" | custom-call | tf_op jit(solution)/shard_map/pallas_call | solution.py:326

commit v3 on v2

--- a/solution.py
+++ b/solution.py
@@ -8,7 +8,6 @@
 from jax.sharding import PartitionSpec as P
 
 MESH = pl.DeviceIdType.MESH
-PIECES = 2
 LIMIT = 40
 
 
@@ -17,6 +16,10 @@
     while ny * 2 * ny * 2 <= fs:
         ny *= 2
     return fs // ny, ny
+
+
+def pieces_of(rows):
+    return max(2, rows // 64)
 
 
 def turns(rows):
@@ -39,10 +42,11 @@
            w_send, w_recv, n_send, n_recv, p_send, p_recv):
     fs = nz * ny
     rows, width = up_f.shape
+    pieces = pieces_of(rows)
     tile = 256
     turned = turns(rows)
     down_all = down_scratch if turned else down_out
-    piece = rows // PIECES
+    piece = rows // pieces
     tokens = prompt.shape[0]
     me = lax.axis_index("fs")
     t = lax.axis_index("tp")
@@ -50,7 +54,7 @@
     exists = (z < nz - 1, z > 0, y < ny - 1, y > 0)
     step = (ny, -ny, 1, -1)
     trick = ny == 2 and nz % 2 == 0
-    half = PIECES // 2
+    half = pieces // 2
     even = lax.rem(z, 2) == 0
     mate = z + 1 - 2 * lax.rem(z, 2)
     buffers = (up_all, down_all)
@@ -67,7 +71,7 @@
     def weights(phase, block, c, direction):
         start = pl.multiple_of(block * rows + c * piece, piece)
         ref = buffers[phase].at[pl.ds(start, piece)]
-        slot = (phase * fs + block) * PIECES + c
+        slot = (phase * fs + block) * pieces + c
         return pltpu.make_async_remote_copy(
             src_ref=ref, dst_ref=ref,
             send_sem=w_send.at[direction, slot], recv_sem=w_recv.at[slot],
@@ -86,13 +90,13 @@
         def _():
             weights(phase, block, c, 0).wait_recv()
 
-    for c in range(PIECES):
+    for c in range(pieces):
         where = pl.ds(pl.multiple_of(me * rows + c * piece, piece), piece)
         part = slice(c * piece, (c + 1) * piece)
         up_all[where, :] = (gain[part, :] * up_f[part, :]).astype(jnp.bfloat16)
     pl.semaphore_wait(barrier, sum(e.astype(jnp.int32) for e in exists) + tp - 1)
     always = z >= 0
-    for c in range(PIECES):
+    for c in range(pieces):
         for direction in range(4):
             send(always, 0, me, c, direction)
 
@@ -100,7 +104,7 @@
     scale = lax.rsqrt(jnp.mean(values * values, axis=-1, keepdims=True) + 1e-06)
     mine = pl.ds(pl.multiple_of(t * tokens, tokens), tokens)
     norm_all[mine, :] = (values * scale).astype(jnp.bfloat16)
-    for c in range(PIECES):
+    for c in range(pieces):
         where = pl.ds(pl.multiple_of(me * rows + c * piece, piece), piece)
         part = slice(c * piece, (c + 1) * piece)
         down_all[where, :] = down_f[part, :].astype(jnp.bfloat16)
@@ -125,12 +129,12 @@
             send(always, 1, me, c, direction)
 
     def own_down(d):
-        for c in range(PIECES):
+        for c in range(pieces):
             send(z == d, 1, me, c, 0)
             send(z == nz - 1 - d, 1, me, c, 1)
 
     def column(phase, d):
-        for c in range(PIECES):
+        for c in range(pieces):
             for s in (1, -1):
                 zb = z + s * d
                 there = jnp.logical_and(zb >= 0, zb < nz)
@@ -147,7 +151,7 @@
         if not trick:
             return
         block = z * ny + 1 - y
-        for c in range(half, PIECES):
+        for c in range(half, pieces):
             if phase == 0:
                 arrive(always, phase, block, c)
             send(even, phase, block, c, 0)
@@ -160,7 +164,7 @@
             for u in (1, -1):
                 yb = y + u * e
                 there = jnp.logical_and(inside, jnp.logical_and(yb >= 0, yb < ny))
-                for c in range(PIECES):
+                for c in range(pieces):
                     if trick and phase == 0 and d == 0 and c >= half:
                         continue
                     wanted = there
@@ -172,7 +176,7 @@
 
     def swapped(phase):
         if trick:
-            for c in range(half, PIECES):
+            for c in range(half, pieces):
                 arrive(always, phase, mate * ny + 1 - y, c)
 
     def partial_copy(block, offset):
@@ -223,7 +227,7 @@
         if d == 1:
             swap(0)
         own_down(d)
-    for c in range(half, PIECES):
+    for c in range(half, pieces):
         for direction in (2, 3):
             send(always, 1, me, c, direction)
     for d in range(nz):
@@ -294,7 +298,7 @@
         bf16 = jnp.bfloat16
         turned = turns(rows)
         down_shape = (width, depth) if turned else (depth, width)
-        slots = 2 * fs * PIECES
+        slots = 2 * fs * pieces_of(rows)
         any_space = pl.BlockSpec(memory_space=pl.ANY)
         vmem = pl.BlockSpec(memory_space=pltpu.VMEM)
         up_whole, down_whole, mixed = pl.pallas_call(

time: 183 us -> 184 us (level)
  Pallas kernels: 180 us -> 182 us
where the time goes in v3:
time: 184 us
  Pallas kernels  182 us (99%)
    pallas_call x1, Pallas kernels, shards(): pl.pallas_call(functools.partial(kernel, nz, ny, tp), out_shape=(pltpu.VM...  176 us
    pallas_call x1, Pallas kernels, shards(): pl.pallas_call(flush, out_shape=(jax.ShapeDtypeStruct((depth, width), bf1...  6.19 us

profile of v3, /device:TPU:1, one launch (start us, length us, event | category | flops | bytes accessed | tf_op | source)
XLA Modules:
  0.0 183.8 jit_solution(12690601289105472558)
XLA Ops:
  0.6 1.5 copy.7.gain
  2.1 175.5 %shard_map.67 = (bf16[2048,2048]{1,0:T(8,128)(2,1)S(1)}, bf16[2048,2048]{1,0:T(8,128)(2,1)S(1)}, bf16[128,2048]{1,0:T(8,128)(2,1)S(1)}) custom-call(bf16[128,2048]{1,0:T(8,128)(2,1)} %prompt.1, f32[256,1]{1,0:T(8,128)} %copy.7.gain, f32[256,2048]{1,0:T(8,128)} %up_f.1, f32[256,2048]{1,0:T(8,128)} %down_f.1), custom_call_target="tpu_custom_call" | custom-call | tf_op jit(solution)/shard_map/pallas_call | solution.py:304
  177.6 6.2 %shard_map.68 = (bf16[2048,2048]{1,0:T(8,128)(2,1)}, bf16[2048,2048]{1,0:T(8,128)(2,1)}, bf16[128,2048]{1,0:T(8,128)(2,1)}) custom-call(bf16[2048,2048]{1,0:T(8,128)(2,1)S(1)} %get-tuple-element.6.up_in, bf16[2048,2048]{1,0:T(8,128)(2,1)S(1)} %get-tuple-element.7.down_in, bf16[128,2048]{1,0:T(8,128)(2,1)S(1)} %get-tuple-element.8.mixed_in), custom_call_target="tpu_custom_call" | custom-call | tf_op jit(solution)/shard_map/pallas_call | solution.py:330
